TPU v7x, 32 devices: a whole 2x2x4 slice. The times are simulated.
32 devices in a mesh: rep: 2 (over x), fs: 4 (over y, core), tp: 4 (over z).
Axes of the slice: x: 2, y: 2, z: 4, core: 2. Of those that a mesh axis runs over, the one named last changes fastest.
Arguments:
- acts: bfloat16 [2048, 2048], P(('rep', 'fs'), 'tp'), may hold values from -6 to 6
- cotangent: bfloat16 [2048, 2048], P(('rep', 'fs'), 'tp'), may hold values from -8 to 8
- pre_act: bfloat16 [2048, 4096], P(('rep', 'fs'), 'tp'), may hold values from -6 to 6
- up_store: float32 [2048, 4096], P('fs', 'tp'), may hold values from -0.125 to 0.125
- up_scale: float32 [4096], P('tp'), may hold values from 0.5 to 2
- down_store: float32 [4096, 2048], P('tp', 'fs'), may hold values from -0.09375 to 0.09375
- down_scale: float32 [2048], replicated, may hold values from 0.5 to 2
Outputs:
- grad_input: bfloat16 [2048, 2048], P(('rep', 'fs'), 'tp')
- grad_up: float32 [2048, 4096], P('fs', 'tp')
- grad_down: float32 [4096, 2048], P('tp', 'fs')
All inputs are finite; a program needn't handle non-finite values.
Results may differ from a plain program's by a relative error of at most 0.007.
Values may be sent and summed in bfloat16 or wider, within the bound.
No kernel may reach another device: no remote copies, remote signals or barrier semaphores. Data moves between devices by JAX's collectives and lax.ppermute only.
A program may use at most 128 MiB of HBM per device.

v0:
```python
import math
import jax
import jax.numpy as jnp
from jax import lax
from jax.sharding import PartitionSpec as P


def contract_last(left, right):
    return lax.dot_general(
        left, right, (((1,), (1,)), ((), ())), preferred_element_type=jnp.float32
    )


def contract_first(left, right):
    return lax.dot_general(
        left, right, (((0,), (0,)), ((), ())), preferred_element_type=jnp.float32
    )


def body(acts, cotangent, pre_act, up_store, up_scale, down_store, down_scale):
    tok_rows = acts.shape[0]
    norm_factor = 1.0 / math.sqrt(tok_rows * lax.axis_size("fs") * lax.axis_size("rep"))
    full_acts, full_cot = (
        lax.all_gather(acts, "tp", axis=1, tiled=True),
        lax.all_gather(cotangent, "tp", axis=1, tiled=True),
    )
    scaled = (full_cot.astype(jnp.float32) * down_scale[None, :]).astype(jnp.bfloat16)
    down_bf = down_store.astype(jnp.bfloat16)
    up_bf = up_store.astype(jnp.bfloat16)
    d_act = contract_last(scaled, lax.all_gather(down_bf, "fs", axis=1, tiled=True))
    positive = jnp.maximum(pre_act.astype(jnp.float32), 0.0)
    act = (positive * positive).astype(jnp.bfloat16)
    d_pre = (2.0 * positive * d_act * up_scale[None, :]).astype(jnp.bfloat16)
    acts_cols, scaled_cols = (
        lax.all_to_all(full_acts, "fs", split_axis=1, concat_axis=0, tiled=True),
        lax.all_to_all(scaled, "fs", split_axis=1, concat_axis=0, tiled=True),
    )
    act_group, dpre_group = (
        lax.all_gather(act, "fs", axis=0, tiled=True),
        lax.all_gather(d_pre, "fs", axis=0, tiled=True),
    )
    grad_down = contract_first(act_group, scaled_cols) * norm_factor
    grad_up = contract_first(acts_cols, dpre_group) * norm_factor
    partial_value = contract_last(d_pre, lax.all_gather(up_bf, "fs", axis=0, tiled=True))
    grad_input = lax.psum_scatter(partial_value, "tp", scatter_dimension=1, tiled=True).astype(
        jnp.bfloat16
    )
    grad_up, grad_down = lax.psum((grad_up, grad_down), "rep")
    return (grad_input, grad_up, grad_down)


def solution(mesh):
    return jax.shard_map(
        body,
        mesh=mesh,
        in_specs=(
            P(("rep", "fs"), "tp"),
            P(("rep", "fs"), "tp"),
            P(("rep", "fs"), "tp"),
            P("fs", "tp"),
            P("tp"),
            P("tp", "fs"),
            P(),
        ),
        out_specs=(P(("rep", "fs"), "tp"), P("fs", "tp"), P("tp", "fs")),
        check_vma=False,
    )
```

profile of v0, /device:TPU:0, one launch (start us, length us, event | category | flops | bytes accessed | tf_op | source)
XLA Modules:
  0.0 364.8 jit_solution(4651438372138626492)
XLA Ops:
  7.2 0.0 all-gather.7.cloned.1.call-start
  7.2 1.8 copy.12
  9.0 0.0 all-gather.7.cloned.1.call-update
  9.0 0.0 copy-start
  9.0 0.0 all-gather.9.cloned.1.call-start
  9.1 2.8 convert_element_type.27
  11.9 0.0 all-gather.9.cloned.1.call-update
  11.9 0.0 copy-start.3
  12.0 0.0 copy-start.2
  12.0 0.0 all-gather.11.cloned.1.call-start
  12.0 0.0 copy-done
  12.0 1.2 convert_element_type.29
  13.2 0.0 copy-start.4
  13.2 0.0 all-gather.11.cloned.1.call-update
  13.2 0.0 all-gather.15.cloned.1.call-start
  13.3 0.0 copy-done.3
  13.3 0.8 copy.13
  14.1 0.0 copy-start.5
  14.1 0.0 all-gather.15.cloned.1.call-update
  14.2 0.0 all-gather.17.cloned.1.call-start
  14.2 0.0 copy-done.2
  14.2 0.9 multiply_convert_fusion.1
  15.1 0.0 all-gather.17.cloned.1.call-update
  15.2 0.0 all-gather.13.cloned.1.call-start
  15.2 25.6 %all-gather.7.cloned.1.call-done = bf16[256,2048]{0,1:T(8,128)(2,1)} async-done(((bf16[256,512]{0,1:T(8,128)(2,1)}), bf16[256,2048]{0,1:T(8,128)(2,1)}) %all-gather.7.cloned.1.call-update) | async-done | bytes 1048592 | tf_op jit(solution)/shard_map/all_gather | solution.py:25
  40.9 0.0 copy-done.4
  40.9 2.5 multiply_convert_fusion
  43.4 33.5 %all-gather.9.cloned.1.call-done = bf16[1024,2048]{1,0:T(8,128)(2,1)} async-done(((bf16[1024,512]{1,0:T(8,128)(2,1)}), bf16[1024,2048]{1,0:T(8,128)(2,1)}) %all-gather.9.cloned.1.call-update) | async-done | bytes 4194320 | tf_op jit(solution)/shard_map/all_gather | solution.py:30
  76.9 0.0 copy-done.5
  76.9 4.7 %fusion.1 = bf16[256,1024]{1,0:T(8,128)(2,1)} fusion(bf16[256,2048]{0,1:T(8,128)(2,1)} %multiply_convert_fusion, bf16[1024,2048]{1,0:T(8,128)(2,1)} %all-gather.9.cloned.1.call-done, bf16[256,1024]{1,0:T(8,128)(2,1)S(1)} %copy-done.2, f32[1024]{0:T(1024)S(1)} %copy-done.5), kind=kOutput, calls=%fused_computation.5 | convolution fusion | flops 1075314688 | bytes 6295552 | tf_op jit(solution)/shard_map/dot_general | solution.py:9
  81.6 0.0 all-gather.13.cloned.1.call-update
  81.6 0.0 reduce-scatter.2.cloned.1.call-start
  81.7 31.2 %all-gather.11.cloned.1.call-done = bf16[2048,1024]{1,0:T(8,128)(2,1)} async-done(((bf16[512,1024]{1,0:T(8,128)(2,1)}), bf16[2048,1024]{1,0:T(8,128)(2,1)}) %all-gather.11.cloned.1.call-update) | async-done | bytes 4194320 | tf_op jit(solution)/shard_map/all_gather | solution.py:44
  112.9 5.0 %fusion.2 = f32[256,2048]{1,0:T(8,128)} fusion(bf16[256,1024]{1,0:T(8,128)(2,1)} %fusion.1, bf16[2048,1024]{1,0:T(8,128)(2,1)} %all-gather.11.cloned.1.call-done), kind=kOutput, calls=%fused_computation.8 | convolution fusion | flops 1073741824 | bytes 6815744 | tf_op jit(solution)/shard_map/dot_general | solution.py:9
  117.9 0.0 reduce-scatter.2.cloned.1.call-update
  117.9 24.4 %all-gather.15.cloned.1.call-done = bf16[256,2048]{0,1:T(8,128)(2,1)} async-done(((bf16[256,512]{0,1:T(8,128)(2,1)}), bf16[256,2048]{0,1:T(8,128)(2,1)}) %all-gather.15.cloned.1.call-update) | async-done | bytes 1048592 | tf_op jit(solution)/shard_map/all_gather | solution.py:24
  142.4 25.7 %all_to_all.38 = bf16[256,4,512]{0,2,1:T(8,128)(2,1)S(1)} all-to-all(bf16[256,4,512]{0,2,1:T(8,128)(2,1)} %bitcast.18), channel_id=1, replica_groups=mesh['rep'=2,'fs'=4,'tp'=4] {'fs'}, dimensions={1} | all-to-all | bytes 2097152 | tf_op jit(solution)/shard_map/all_to_all | solution.py:35
  168.1 3.5 all-to-all-start.1
  171.6 0.0 all-reduce.3.cloned.1.call-start
  171.7 0.5 copy.14
  172.2 17.6 %all-to-all-done.1 = bf16[256,4,512]{0,2,1:T(8,128)(2,1)S(1)} async-done(((bf16[256,4,512]{0,2,1:T(8,128)(2,1)}), bf16[256,4,512]{0,2,1:T(8,128)(2,1)S(1)}, u32[]{:S(2)}, u32[]{:S(2)}) %all-to-all-start.1) | async-done | bytes 1048608 | tf_op jit(solution)/shard_map/all_to_all | solution.py:36
  189.8 0.5 copy.15
  190.3 0.0 all-gather.17.cloned.1.call-done
  190.4 4.3 %convolution_multiply_fusion = f32[1024,512]{1,0:T(8,128)} fusion(bf16[1024,1024]{1,0:T(8,128)(2,1)} %all-gather.17.cloned.1.call-done, bf16[1024,512]{1,0:T(8,128)(2,1)S(1)} %bitcast.20), kind=kOutput, calls=%fused_computation.2 | convolution fusion | flops 1074266112 | bytes 5242880 | tf_op jit(solution)/shard_map/dot_general | solution.py:15
  194.7 4.1 %all-gather.13.cloned.1.call-done = bf16[1024,1024]{1,0:T(8,128)(2,1)} async-done(((bf16[256,1024]{1,0:T(8,128)(2,1)}), bf16[1024,1024]{1,0:T(8,128)(2,1)}) %all-gather.13.cloned.1.call-update) | async-done | bytes 2097168 | tf_op jit(solution)/shard_map/all_gather | solution.py:40
  198.8 4.2 %multiply_bitcast_fusion = f32[512,1024]{0,1:T(8,128)} fusion(bf16[1024,1024]{1,0:T(8,128)(2,1)} %all-gather.13.cloned.1.call-done, bf16[1024,512]{1,0:T(8,128)(2,1)S(1)} %bitcast.19), kind=kOutput, calls=%fused_computation | convolution fusion | flops 1074266112 | bytes 5242880 | tf_op jit(solution)/shard_map/dot_general | solution.py:15
  203.0 0.0 all-reduce.3.cloned.1.call-update
  203.0 40.4 %reduce-scatter.2.cloned.1.call-done = f32[256,512]{1,0:T(8,128)} async-done(((f32[256,2048]{1,0:T(8,128)}), f32[256,512]{1,0:T(8,128)}) %reduce-scatter.2.cloned.1.call-update) | async-done | bytes 524304 | tf_op jit(solution)/shard_map/reduce_scatter | solution.py:45
  243.4 1.8 convert_element_type.30
  245.1 108.4 %all-reduce.3.cloned.1.call-done = (f32[512,1024]{0,1:T(8,128)}, f32[1024,512]{1,0:T(8,128)}) async-done(((f32[512,1024]{0,1:T(8,128)}, f32[1024,512]{1,0:T(8,128)}), (f32[512,1024]{0,1:T(8,128)}, f32[1024,512]{1,0:T(8,128)})) %all-reduce.3.cloned.1.call-update) | async-done | bytes 4194320 | tf_op jit(solution)/shard_map/psum | solution.py:48
  353.6 0.0 copy-start.1
  353.6 3.0 copy.16
  356.6 0.0 copy-done.1
  356.6 1.3 copy.19
Async XLA Ops:
  7.2 33.7 %all-gather.7.cloned.1.call-start = ((), (), s32[]{:S(2)}) async-start(), calls=%async_computation.3 | async-start | bytes 1310720 | tf_op jit(solution)/shard_map/all_gather | solution.py:25
  9.0 3.0 copy-start
  9.0 67.8 %all-gather.9.cloned.1.call-start = ((), (), s32[]{:S(2)}) async-start(), calls=%async_computation.4 | async-start | bytes 5242880 | tf_op jit(solution)/shard_map/all_gather | solution.py:30
  11.9 1.3 copy-start.3
  12.0 2.2 copy-start.2
  12.0 100.9 %all-gather.11.cloned.1.call-start = ((), (), s32[]{:S(2)}) async-start(), calls=%async_computation.5 | async-start | bytes 5242880 | tf_op jit(solution)/shard_map/all_gather | solution.py:44
  13.2 27.7 %copy-start.4 = (f32[2048]{0:T(1024)S(1)}, f32[2048]{0:T(1024)}, u32[]{:S(2)}) copy-start(f32[2048]{0:T(1024)} %param.13) | copy-start | bytes 24580
  13.2 129.1 %all-gather.15.cloned.1.call-start = ((), (), s32[]{:S(2)}) async-start(), calls=%async_computation.8 | async-start | bytes 1310720 | tf_op jit(solution)/shard_map/all_gather | solution.py:24
  14.1 62.7 %copy-start.5 = (f32[1024]{0:T(1024)S(1)}, f32[1024]{0:T(1024)}, u32[]{:S(2)}) copy-start(f32[1024]{0:T(1024)} %param.11) | copy-start | bytes 12292
  14.2 176.2 %all-gather.17.cloned.1.call-start = ((), (), s32[]{:S(2)}) async-start(), calls=%async_computation.9 | async-start | bytes 2621440 | tf_op jit(solution)/shard_map/all_gather | solution.py:39
  15.2 183.6 %all-gather.13.cloned.1.call-start = ((), (), s32[]{:S(2)}) async-start(), calls=%async_computation.7 | async-start | bytes 2621440 | tf_op jit(solution)/shard_map/all_gather | solution.py:40
  81.6 161.8 %reduce-scatter.2.cloned.1.call-start = ((), (), s32[]{:S(2)}) async-start(), calls=%async_computation.6 | async-start | bytes 2621440 | tf_op jit(solution)/shard_map/reduce_scatter | solution.py:45
  168.1 21.7 %all-to-all-start.1 = ((bf16[256,4,512]{0,2,1:T(8,128)(2,1)}), bf16[256,4,512]{0,2,1:T(8,128)(2,1)S(1)}, u32[]{:S(2)}, u32[]{:S(2)}) async-start(bf16[256,4,512]{0,2,1:T(8,128)(2,1)} %bitcast.4), calls=%async_computation.2 | async-start | bytes 2097152 | tf_op jit(solution)/shard_map/all_to_all | solution.py:36
  171.6 182.0 %all-reduce.3.cloned.1.call-start = ((), (), s32[]{:S(2)}) async-start(), calls=%async_computation.10 | async-start | bytes 8388608 | tf_op jit(solution)/shard_map/psum | solution.py:48
  353.6 3.0 copy-start.1
Sparse Core Ops, SparseCore 0:
  10.1 30.6 all-gather.6
  43.0 33.8 all-gather.8
  78.4 34.4 all-gather.10
  114.3 27.9 all-gather.14
  143.8 29.3 all-gather.16
  174.5 24.2 all-gather.12
  201.6 41.6 reduce-scatter.1
  246.4 107.1 all-reduce.2
where the time goes:
time: 365 us
  waiting for transfers between devices  285 us (78%)
  blocking collectives  25.7 us (7%)
  matrix products  18.2 us (5%)
  between operations  14.2 us (4%)
  other arithmetic  9.24 us (3%)
  local copies, waits for them, and re-layouts  8.09 us (2%)
  starting transfers between devices  3.85 us (1%)
    psum x1, waiting for transfers between devices, body(): grad_up, grad_down = lax.psum((grad_up, grad_down), 'rep')  108 us
    reduce_scatter x1, waiting for transfers between devices, body(): lax.psum_scatter(partial_value, 'tp', scatter_dimension=1, tiled=True)  40.4 us
    all_gather x1, waiting for transfers between devices, body(): lax.all_gather(down_bf, 'fs', axis=1, tiled=True)  33.5 us
    all_gather x1, waiting for transfers between devices, body(): lax.all_gather(up_bf, 'fs', axis=0, tiled=True)  31.2 us
    all_to_all x1, blocking collectives, body(): lax.all_to_all(full_acts, 'fs', split_axis=1, concat_axis=0, tiled=True)  25.7 us
    all_gather x1, waiting for transfers between devices, body(): lax.all_gather(cotangent, 'tp', axis=1, tiled=True)  25.6 us
    all_gather x1, waiting for transfers between devices, body(): lax.all_gather(acts, 'tp', axis=1, tiled=True)  24.4 us
    all_to_all x1, waiting for transfers between devices, body(): lax.all_to_all(scaled, 'fs', split_axis=1, concat_axis=0, tiled=True)  17.6 us
  transfers between devices with their start and end apart: 9, of which 8 were waited for; matrix products, arithmetic and copies ran while one was open for 8% of the time, Pallas kernels for 0%

commit v1 on v0

--- a/solution.py
+++ b/solution.py
@@ -3,6 +3,13 @@
 import jax.numpy as jnp
 from jax import lax
 from jax.sharding import PartitionSpec as P
+from jax.lax import all_to_all, axis_size
+
+
+def extend_the_cells(named_axis, mat):
+    return jnp.concatenate(
+        all_to_all(jnp.stack(axis_size(named_axis) * [mat], 0), named_axis, 0, 0), 1
+    )
 
 
 def contract_last(left, right):
@@ -21,7 +28,7 @@
     tok_rows = acts.shape[0]
     norm_factor = 1.0 / math.sqrt(tok_rows * lax.axis_size("fs") * lax.axis_size("rep"))
     full_acts, full_cot = (
-        lax.all_gather(acts, "tp", axis=1, tiled=True),
+        extend_the_cells("tp", acts),
         lax.all_gather(cotangent, "tp", axis=1, tiled=True),
     )
     scaled = (full_cot.astype(jnp.float32) * down_scale[None, :]).astype(jnp.bfloat16)

time: 365 us -> 336 us (0.921)
  waiting for transfers between devices: 285 us -> 232 us
  blocking collectives: 25.7 us -> 51.7 us
    all_to_all x1 -> x2, blocking collectives: 25.7 us -> 51.7 us  [the longest x1 30.6 us: extend_the_cells(): all_to_all(jnp.stack(axis_size(named_axis) * [mat], 0), named_axis, 0, 0)]
    all_gather x1 -> x0, waiting for transfers between devices: 24.4 us -> none  [body(): lax.all_gather(acts, 'tp', axis=1, tiled=True)]
    reduce_scatter x1, waiting for transfers between devices: 40.4 us -> 21 us  [body(): lax.psum_scatter(partial_value, 'tp', scatter_dimension=1, tiled=True)]
    all_to_all x1, waiting for transfers between devices: 17.6 us -> 9.3 us  [body(): lax.all_to_all(full_acts, 'fs', split_axis=1, concat_axis=0, tiled=True)]
    all_gather x1, waiting for transfers between devices: 4.1 us -> 0.01 us  [body(): lax.all_gather(d_pre, 'fs', axis=0, tiled=True)]
  transfers between devices with their start and end apart: 9 -> 8, of which waited for: 8 -> 6; matrix products, arithmetic and copies ran while one was open for 8% -> 8% of each run, Pallas kernels for 0% -> 0%
where the time goes in v1:
time: 336 us
  waiting for transfers between devices  232 us (69%)
  blocking collectives  51.7 us (15%)
  matrix products  18 us (5%)
  between operations  14.2 us (4%)
  other arithmetic  8.22 us (2%)
  local copies, waits for them, and re-layouts  7.71 us (2%)
  starting transfers between devices  3.8 us (1%)
    psum x1, waiting for transfers between devices, body(): grad_up, grad_down = lax.psum((grad_up, grad_down), 'rep')  108 us
    all_gather x1, waiting for transfers between devices, body(): lax.all_gather(down_bf, 'fs', axis=1, tiled=True)  34.4 us
    all_gather x1, waiting for transfers between devices, body(): lax.all_gather(up_bf, 'fs', axis=0, tiled=True)  32.2 us
    all_to_all x1, blocking collectives, extend_the_cells(): all_to_all(jnp.stack(axis_size(named_axis) * [mat], 0), named_axis, 0, 0)  30.6 us
    all_gather x1, waiting for transfers between devices, body(): lax.all_gather(cotangent, 'tp', axis=1, tiled=True)  26.6 us
    all_to_all x1, blocking collectives, body(): lax.all_to_all(scaled, 'fs', split_axis=1, concat_axis=0, tiled=True)  21.1 us
    reduce_scatter x1, waiting for transfers between devices, body(): lax.psum_scatter(partial_value, 'tp', scatter_dimension=1, tiled=True)  21 us
    dot_general x2, matrix products, contract_last(): lax.dot_general(left, right, (((1,), (1,)), ((), ())), preferred_element_...  9.31 us
  transfers between devices with their start and end apart: 8, of which 6 were waited for; matrix products, arithmetic and copies ran while one was open for 8% of the time, Pallas kernels for 0%

profile of v1, /device:TPU:0, one launch (start us, length us, event | category | flops | bytes accessed | tf_op | source)
XLA Modules:
  0.0 335.7 jit_solution(15512065897621359785)
XLA Ops:
  7.2 0.0 all-gather.6.cloned.1.call-start
  7.2 1.8 copy.12
  9.0 0.0 all-gather.6.cloned.1.call-update
  9.0 0.0 copy-start
  9.0 0.0 all-gather.8.cloned.1.call-start
  9.1 2.8 convert_element_type.27
  11.9 0.0 all-gather.8.cloned.1.call-update
  11.9 0.0 copy-start.2
  12.0 0.0 all-gather.10.cloned.1.call-start
  12.0 0.0 copy-done
  12.0 1.1 convert_element_type.29
  13.2 0.0 copy-start.4
  13.2 0.0 all-gather.10.cloned.1.call-update
  13.2 0.0 copy-start.5
  13.2 0.0 all-gather.14.cloned.1.call-start
  13.2 0.0 copy-done.2
  13.3 0.9 multiply_convert_fusion.1
  14.2 0.0 all-gather.14.cloned.1.call-update
  14.2 0.0 all-gather.12.cloned.1.call-start
  14.2 26.6 %all-gather.6.cloned.1.call-done = bf16[256,2048]{0,1:T(8,128)(2,1)} async-done(((bf16[256,512]{0,1:T(8,128)(2,1)}), bf16[256,2048]{0,1:T(8,128)(2,1)}) %all-gather.6.cloned.1.call-update) | async-done | bytes 1048592 | tf_op jit(solution)/shard_map/all_gather | solution.py:32
  40.9 0.0 copy-done.4
  40.9 1.6 multiply_convert_fusion
  42.4 34.4 %all-gather.8.cloned.1.call-done = bf16[1024,2048]{1,0:T(8,128)(2,1)} async-done(((bf16[1024,512]{1,0:T(8,128)(2,1)}), bf16[1024,2048]{1,0:T(8,128)(2,1)}) %all-gather.8.cloned.1.call-update) | async-done | bytes 4194320 | tf_op jit(solution)/shard_map/all_gather | solution.py:37
  76.9 0.0 copy-done.5
  76.9 4.4 %fusion.1 = bf16[256,1024]{1,0:T(8,128)(2,1)} fusion(bf16[256,2048]{0,1:T(8,128)(2,1)S(1)} %multiply_convert_fusion, bf16[1024,2048]{1,0:T(8,128)(2,1)} %all-gather.8.cloned.1.call-done, bf16[256,1024]{1,0:T(8,128)(2,1)S(1)} %copy-done.2, f32[1024]{0:T(1024)S(1)} %copy-done.5), kind=kOutput, calls=%fused_computation.5 | convolution fusion | flops 1075314688 | bytes 6295552 | tf_op jit(solution)/shard_map/dot_general | solution.py:16
  81.2 0.0 all-gather.12.cloned.1.call-update
  81.2 0.0 reduce-scatter.2.cloned.1.call-start
  81.3 32.2 %all-gather.10.cloned.1.call-done = bf16[2048,1024]{1,0:T(8,128)(2,1)} async-done(((bf16[512,1024]{1,0:T(8,128)(2,1)}), bf16[2048,1024]{1,0:T(8,128)(2,1)}) %all-gather.10.cloned.1.call-update) | async-done | bytes 4194320 | tf_op jit(solution)/shard_map/all_gather | solution.py:51
  113.5 5.0 %fusion.2 = f32[256,2048]{1,0:T(8,128)} fusion(bf16[256,1024]{1,0:T(8,128)(2,1)} %fusion.1, bf16[2048,1024]{1,0:T(8,128)(2,1)} %all-gather.10.cloned.1.call-done), kind=kOutput, calls=%fused_computation.8 | convolution fusion | flops 1073741824 | bytes 6815744 | tf_op jit(solution)/shard_map/dot_general | solution.py:16
  118.5 0.0 copy-start.3
  118.5 0.0 reduce-scatter.2.cloned.1.call-update
  118.5 0.9 copy-done.3
  119.4 0.1 stack.2
  119.5 30.6 %all_to_all.40 = bf16[4,256,512]{2,1,0:T(8,128)(2,1)} all-to-all(bf16[4,256,512]{2,1,0:T(8,128)(2,1)S(1)} %stack.2), channel_id=1, replica_groups=mesh['rep'=2,'fs'=4,'tp'=4] {'tp'}, dimensions={0} | all-to-all | bytes 2097152 | tf_op jit(solution)/shard_map/all_to_all | solution.py:11
  150.1 21.1 %all_to_all.41 = bf16[256,4,512]{0,2,1:T(8,128)(2,1)S(1)} all-to-all(bf16[256,4,512]{0,2,1:T(8,128)(2,1)S(1)} %bitcast.17), channel_id=1, replica_groups=mesh['rep'=2,'fs'=4,'tp'=4] {'fs'}, dimensions={1} | all-to-all | bytes 2097152 | tf_op jit(solution)/shard_map/all_to_all | solution.py:43
  171.2 3.5 %all-to-all-start.1 = ((bf16[256,4,512]{2,0,1:T(8,128)(2,1)}), bf16[256,4,512]{2,0,1:T(8,128)(2,1)S(1)}, u32[]{:S(2)}, u32[]{:S(2)}) async-start(bf16[256,4,512]{2,0,1:T(8,128)(2,1)} %bitcast), calls=%async_computation.2 | async-start | bytes 2097152 | tf_op jit(solution)/shard_map/all_to_all | solution.py:42
  174.7 0.0 all-reduce.3.cloned.1.call-start
  174.8 0.5 copy.13
  175.3 0.0 all-gather.14.cloned.1.call-done
  175.4 4.5 %convolution_multiply_fusion = f32[1024,512]{1,0:T(8,128)} fusion(bf16[1024,1024]{1,0:T(8,128)(2,1)} %all-gather.14.cloned.1.call-done, bf16[1024,512]{1,0:T(8,128)(2,1)S(1)} %bitcast.20), kind=kOutput, calls=%fused_computation.2 | convolution fusion | flops 1074266112 | bytes 5242880 | tf_op jit(solution)/shard_map/dot_general | solution.py:22
  179.8 9.3 %all-to-all-done.1 = bf16[256,4,512]{2,0,1:T(8,128)(2,1)S(1)} async-done(((bf16[256,4,512]{2,0,1:T(8,128)(2,1)}), bf16[256,4,512]{2,0,1:T(8,128)(2,1)S(1)}, u32[]{:S(2)}, u32[]{:S(2)}) %all-to-all-start.1) | async-done | bytes 1048608 | tf_op jit(solution)/shard_map/all_to_all | solution.py:42
  189.1 0.0 all-gather.12.cloned.1.call-done
  189.1 4.2 %multiply_bitcast_fusion = f32[512,1024]{0,1:T(8,128)} fusion(bf16[1024,1024]{1,0:T(8,128)(2,1)} %all-gather.12.cloned.1.call-done, bf16[1024,512]{1,0:T(8,128)(2,1)S(1)} %bitcast.19), kind=kOutput, calls=%fused_computation | convolution fusion | flops 1074266112 | bytes 5242880 | tf_op jit(solution)/shard_map/dot_general | solution.py:22
  193.3 0.0 all-reduce.3.cloned.1.call-update
  193.4 21.0 %reduce-scatter.2.cloned.1.call-done = f32[256,512]{1,0:T(8,128)} async-done(((f32[256,2048]{1,0:T(8,128)}), f32[256,512]{1,0:T(8,128)}) %reduce-scatter.2.cloned.1.call-update) | async-done | bytes 524304 | tf_op jit(solution)/shard_map/reduce_scatter | solution.py:52
  214.3 1.8 convert_element_type.30
  216.1 108.4 %all-reduce.3.cloned.1.call-done = (f32[512,1024]{0,1:T(8,128)}, f32[1024,512]{1,0:T(8,128)}) async-done(((f32[512,1024]{0,1:T(8,128)}, f32[1024,512]{1,0:T(8,128)}), (f32[512,1024]{0,1:T(8,128)}, f32[1024,512]{1,0:T(8,128)})) %all-reduce.3.cloned.1.call-update) | async-done | bytes 4194320 | tf_op jit(solution)/shard_map/psum | solution.py:55
  324.5 0.0 copy-start.1
  324.5 3.0 copy.14
  327.6 0.0 copy-done.1
  327.6 1.3 copy.17
Async XLA Ops:
  7.2 33.7 %all-gather.6.cloned.1.call-start = ((), (), s32[]{:S(2)}) async-start(), calls=%async_computation.4 | async-start | bytes 1310720 | tf_op jit(solution)/shard_map/all_gather | solution.py:32
  9.0 3.0 copy-start
  9.0 67.8 %all-gather.8.cloned.1.call-start = ((), (), s32[]{:S(2)}) async-start(), calls=%async_computation.5 | async-start | bytes 5242880 | tf_op jit(solution)/shard_map/all_gather | solution.py:37
  11.9 1.3 copy-start.2
  12.0 101.5 %all-gather.10.cloned.1.call-start = ((), (), s32[]{:S(2)}) async-start(), calls=%async_computation.6 | async-start | bytes 5242880 | tf_op jit(solution)/shard_map/all_gather | solution.py:51
  13.2 27.7 %copy-start.4 = (f32[2048]{0:T(1024)S(1)}, f32[2048]{0:T(1024)}, u32[]{:S(2)}) copy-start(f32[2048]{0:T(1024)} %param.13) | copy-start | bytes 24580
  13.2 63.7 %copy-start.5 = (f32[1024]{0:T(1024)S(1)}, f32[1024]{0:T(1024)}, u32[]{:S(2)}) copy-start(f32[1024]{0:T(1024)} %param.11) | copy-start | bytes 12292
  13.2 162.2 %all-gather.14.cloned.1.call-start = ((), (), s32[]{:S(2)}) async-start(), calls=%async_computation.9 | async-start | bytes 2621440 | tf_op jit(solution)/shard_map/all_gather | solution.py:46
  14.2 174.9 %all-gather.12.cloned.1.call-start = ((), (), s32[]{:S(2)}) async-start(), calls=%async_computation.8 | async-start | bytes 2621440 | tf_op jit(solution)/shard_map/all_gather | solution.py:47
  81.2 133.1 %reduce-scatter.2.cloned.1.call-start = ((), (), s32[]{:S(2)}) async-start(), calls=%async_computation.7 | async-start | bytes 2621440 | tf_op jit(solution)/shard_map/reduce_scatter | solution.py:52
  118.5 0.9 copy-start.3
  171.2 17.9 %all-to-all-start.1 = ((bf16[256,4,512]{2,0,1:T(8,128)(2,1)}), bf16[256,4,512]{2,0,1:T(8,128)(2,1)S(1)}, u32[]{:S(2)}, u32[]{:S(2)}) async-start(bf16[256,4,512]{2,0,1:T(8,128)(2,1)} %bitcast), calls=%async_computation.2 | async-start | bytes 2097152 | tf_op jit(solution)/shard_map/all_to_all | solution.py:42
  174.7 149.8 %all-reduce.3.cloned.1.call-start = ((), (), s32[]{:S(2)}) async-start(), calls=%async_computation.10 | async-start | bytes 8388608 | tf_op jit(solution)/shard_map/psum | solution.py:55
  324.5 3.0 copy-start.1
Sparse Core Ops, SparseCore 0:
  10.1 30.6 all-gather.5
  43.0 33.8 all-gather.7
  79.0 34.4 all-gather.9
  114.9 22.5 all-gather.13
  138.9 26.8 all-gather.11
  168.5 45.7 reduce-scatter.1
  217.4 107.1 all-reduce.2
